TPU v7x, 32 devices: a whole 2x2x4 slice. The times are simulated.
32 devices in a mesh: ep: 32 (over z, y, x, core).
Axes of the slice: x: 2, y: 2, z: 4, core: 2. Of those that a mesh axis runs over, the one named last changes fastest.
Arguments:
- tokens: bfloat16 [512, 2048], P('ep'), may hold values from -6 to 6
- cache_keys: bfloat16 [512, 1024, 128], P('ep'), may hold values from -6 to 6
- cache_values: bfloat16 [512, 1024, 128], P('ep'), may hold values from -6 to 6
- cache_len: int32 [512], P('ep'), may hold values from 1 to 1024
- norm_gain_first: float32 [2048], replicated, may hold values from 0.1 to 1.9
- w_query: bfloat16 [2048, 2048], P(None, 'ep'), may hold values from -0.125 to 0.125
- w_key: bfloat16 [2048, 128], replicated, may hold values from -0.125 to 0.125
- w_value: bfloat16 [2048, 128], replicated, may hold values from -0.125 to 0.125
- head_bias: float32 [32], replicated, may hold values from -8.5 to -3
- w_output: bfloat16 [2048, 2048], P(None, 'ep'), may hold values from -0.125 to 0.125
- norm_gain_second: float32 [2048], replicated, may hold values from 0.1 to 1.9
- group_id: int32 [512], P('ep'), may hold values from 0 to 1, as said below
- member: int32 [512, 6], P('ep'), may hold values from 0 to 15, as said below
- group_gate: float32 [512], P('ep'), may hold values from 0.3 to 1
- member_weight: float32 [512, 6], P('ep'), may hold values from 0.05 to 0.5
- expert_gate_w: bfloat16 [32, 2048, 512], P('ep'), may hold values from -0.125 to 0.125
- expert_up_w: bfloat16 [32, 2048, 512], P('ep'), may hold values from -0.125 to 0.125
- expert_down_w: bfloat16 [32, 512, 2048], P('ep'), may hold values from -0.25 to 0.25
- dense_gate_w: bfloat16 [2048, 2048], P(None, 'ep'), may hold values from -0.125 to 0.125
- dense_up_w: bfloat16 [2048, 2048], P(None, 'ep'), may hold values from -1 to 1
- hidden_gain: float32 [2048], replicated, may hold values from 0.1 to 1.9
- dense_down_w: bfloat16 [2048, 2048], P(None, 'ep'), may hold values from -0.125 to 0.125
- branch_logit: float32 [2048], replicated, may hold values from -8 to 8
Outputs:
- mixed_out: bfloat16 [512, 2048], P('ep')
- new_keys: bfloat16 [512, 128], P('ep')
- new_values: bfloat16 [512, 128], P('ep')
Inputs may be any that keep to these rules, and one draw needn't show every extreme that they name: `group_id`: each group number is named by exactly 8 of the tokens of one device. `member`: each row names 6 different members; with group_id, no expert is named by more than 8 tokens of one device, and some expert is named by 8 tokens of every device.
All inputs are finite; a program needn't handle non-finite values.
Results may differ from a plain program's by a relative error of at most 0.0085.
Values may be sent and summed in bfloat16 or wider, within the bound.
A program may use at most 128 MiB of HBM per device.

v0:
```python
import functools
import types

import jax
import jax.numpy as jnp
from jax import lax
from jax.experimental import pallas as pl
from jax.experimental.pallas import tpu as pltpu
from jax.sharding import PartitionSpec as P

HEADS = 32
HEAD_DIM = 64
KV_HEADS = 2
PER_GROUP = 16
TOP_K = 6
LANES = 128
MESH = pl.DeviceIdType.MESH

epsilon = 1e-06


def torus_of(chips):
    best = (chips, 1, 1)
    for x in range(1, chips + 1):
        for y in range(x, chips + 1):
            if chips % (x * y) == 0 and chips // (x * y) >= y:
                z = chips // (x * y)
                if z + y + x < sum(best):
                    best = (z, y, x)
    return best


def rms_scale(values):
    return lax.rsqrt(jnp.mean(values * values, axis=-1, keepdims=True) + epsilon)


class Place:
    def __init__(self, chips):
        self.chips = chips
        self.dims = torus_of(chips)
        me = lax.axis_index("ep")
        self.core = lax.rem(me, 2)
        self.chip = me // 2
        depth, height, width = self.dims
        self.x = lax.rem(self.chip, width)
        self.y = lax.rem(self.chip // width, height)
        self.z = self.chip // (width * height)

    def at(self, dz, dy, dx):
        depth, height, width = self.dims
        z = lax.rem(self.z + dz + depth, depth)
        y = lax.rem(self.y + dy + height, height)
        x = lax.rem(self.x + dx + width, width)
        return (z * height + y) * width + x

    def device(self, chip):
        return (chip * 2 + self.core,)

    def greet(self):
        barrier = pltpu.get_barrier_semaphore()
        for step in range(1, self.chips):
            other = lax.rem(self.chip + step, self.chips)
            pl.semaphore_signal(barrier, inc=1, device_id=self.device(other), device_id_type=MESH)
        pl.semaphore_wait(barrier, self.chips - 1)


def spread(place, halves):
    depth, height, width = place.dims
    sent = []
    counts = [0, 0]

    def push(half, source, origin, target):
        own, slots, send, recv = halves[half]
        copy = pltpu.make_async_remote_copy(
            src_ref=own if source is None else slots.at[source],
            dst_ref=slots.at[origin],
            send_sem=send.at[counts[half]],
            recv_sem=recv.at[origin],
            device_id=place.device(target),
            device_id_type=MESH,
        )
        counts[half] += 1
        copy.start()
        sent.append(copy)

    def arrive(half, origin):
        own, slots, send, recv = halves[half]
        pltpu.make_async_remote_copy(
            src_ref=slots.at[origin],
            dst_ref=slots.at[origin],
            send_sem=send.at[0],
            recv_sem=recv.at[origin],
            device_id=place.device(place.chip),
            device_id_type=MESH,
        ).wait_recv()

    def along(half, source, origin, axis):
        if axis == "x":
            for step in range(1, width):
                push(half, source, origin, place.at(0, 0, step))
        else:
            for step in range(1, height):
                push(half, source, origin, place.at(0, step, 0))

    orders = (("x", "y"), ("y", "x"))
    for step in range(1, depth):
        for half in range(2):
            push(half, None, place.chip, place.at(step, 0, 0))
    for half in range(2):
        for axis in orders[half]:
            along(half, None, place.chip, axis)
    for step in range(1, depth):
        for half in range(2):
            origin = place.at(-step, 0, 0)
            arrive(half, origin)
            for axis in orders[half]:
                along(half, origin, origin, axis)
    for up in range(depth):
        for half in range(2):
            reach = width if half == 0 else height
            for step in range(1, reach):
                origin = place.at(-up, 0, -step) if half == 0 else place.at(-up, -step, 0)
                arrive(half, origin)
                along(half, origin, origin, orders[half][1])
    for up in range(depth):
        for half in range(2):
            for dy in range(height):
                for dx in range(width):
                    if (dy if half == 0 else dx) != 0:
                        arrive(half, place.at(-up, -dy, -dx))
    for half in range(2):
        own, slots, _, _ = halves[half]
        slots[place.chip] = own[...]
    return sent


def deliver(place, tiles, landed, send, recv, out_ref):
    copies = []
    for step in range(1, place.chips):
        other = lax.rem(place.chip + step, place.chips)
        copy = pltpu.make_async_remote_copy(
            src_ref=tiles.at[other],
            dst_ref=landed.at[place.chip],
            send_sem=send.at[step],
            recv_sem=recv.at[place.chip],
            device_id=place.device(other),
            device_id_type=MESH,
        )
        copy.start()
        copies.append(copy)
    landed[place.chip] = tiles[place.chip]
    for step in range(1, place.chips):
        origin = lax.rem(place.chip - step + place.chips, place.chips)
        pltpu.make_async_remote_copy(
            src_ref=landed.at[origin],
            dst_ref=landed.at[origin],
            send_sem=send.at[0],
            recv_sem=recv.at[origin],
            device_id=place.device(place.chip),
            device_id_type=MESH,
        ).wait_recv()
    lanes = landed.shape[2]
    for block in range(place.chips):
        out_ref[:, block * lanes : (block + 1) * lanes] = landed[block]
    for copy in copies:
        copy.wait_send()


def flat(slots):
    count, rows, columns = slots.shape
    return slots[...].reshape(count * rows, columns)


def project_kernel(chips, a_ref, b_ref, w_ref, out_ref, slots_a, slots_b, tiles, landed,
                   send_a, recv_a, send_b, recv_b, send_t, recv_t):
    place = Place(chips)
    place.greet()
    sent = spread(place, ((a_ref, slots_a, send_a, recv_a), (b_ref, slots_b, send_b, recv_b)))
    cut = a_ref.shape[1]
    product = jnp.dot(flat(slots_a), w_ref[:cut], preferred_element_type=jnp.float32)
    product = product + jnp.dot(flat(slots_b), w_ref[cut:], preferred_element_type=jnp.float32)
    tiles[...] = product.astype(jnp.bfloat16).reshape(tiles.shape)
    deliver(place, tiles, landed, send_t, recv_t, out_ref)
    for copy in sent:
        copy.wait_send()


def gather_kernel(chips, a_ref, b_ref, gate_ref, up_ref, rows_ref, notes_ref, hidden_ref, slots_a, slots_b,
                  send_a, recv_a, send_b, recv_b):
    place = Place(chips)
    place.greet()
    sent = spread(place, ((a_ref, slots_a, send_a, recv_a), (b_ref, slots_b, send_b, recv_b)))
    cut = b_ref.shape[1]
    rows_a = slots_a[:, :, :cut].reshape(chips * a_ref.shape[0], cut)
    rows_b = flat(slots_b)
    rows_ref[:, :cut] = rows_a
    rows_ref[:, cut:] = rows_b
    notes_ref[...] = slots_a[:, :, cut:].reshape(notes_ref.shape)
    gate = jnp.dot(rows_a, gate_ref[:cut], preferred_element_type=jnp.float32)
    gate = gate + jnp.dot(rows_b, gate_ref[cut:], preferred_element_type=jnp.float32)
    upper = jnp.dot(rows_a, up_ref[:cut], preferred_element_type=jnp.float32)
    upper = upper + jnp.dot(rows_b, up_ref[cut:], preferred_element_type=jnp.float32)
    hidden_ref[...] = (jax.nn.silu(gate) * upper).astype(jnp.bfloat16)
    for copy in sent:
        copy.wait_send()


def down_kernel(chips, a_ref, b_ref, gain_ref, w_ref, out_ref, slots_a, slots_b, tiles, landed,
                send_a, recv_a, send_b, recv_b, send_t, recv_t):
    place = Place(chips)
    place.greet()
    sent = spread(place, ((a_ref, slots_a, send_a, recv_a), (b_ref, slots_b, send_b, recv_b)))
    rows, lanes = a_ref.shape
    part = chips // 2
    for half, slots in enumerate((slots_a, slots_b)):
        square = jnp.zeros((rows, lanes), jnp.float32)
        for block in range(chips):
            value = slots[block].astype(jnp.float32)
            square = square + value * value
        mean = jnp.sum(square, axis=1, keepdims=True) / (chips * lanes)
        scale = lax.rsqrt(mean + epsilon)
        total = jnp.zeros((rows, lanes), jnp.float32)
        for block in range(chips):
            gain = gain_ref[:, block * lanes : (block + 1) * lanes]
            normed = (slots[block].astype(jnp.float32) * scale * gain).astype(jnp.bfloat16)
            total = total + jnp.dot(
                normed,
                w_ref[block * lanes : (block + 1) * lanes],
                preferred_element_type=jnp.float32,
            )
        tiles[half * part : (half + 1) * part] = total.astype(jnp.bfloat16).reshape(
            part, rows // part, lanes
        )
    deliver(place, tiles, landed, send_t, recv_t, out_ref)
    for copy in sent:
        copy.wait_send()


def whole():
    return pl.BlockSpec(memory_space=pltpu.VMEM)


def spread_scratch(chips, a, b):
    slots = [pltpu.VMEM((chips,) + a.shape, a.dtype), pltpu.VMEM((chips,) + b.shape, b.dtype)]
    return slots, [pltpu.SemaphoreType.DMA((chips,))] * 4


def remote_params(number):
    return pltpu.CompilerParams(collective_id=number, has_side_effects=True)


def project(chips, number, rows, weight):
    count, width = rows.shape
    lanes = weight.shape[1]
    a, b = rows[:, : width // 2], rows[:, width // 2 :]
    slots, sems = spread_scratch(chips, a, b)
    tile = pltpu.VMEM((chips, count, lanes), jnp.bfloat16)
    return pl.pallas_call(
        functools.partial(project_kernel, chips),
        out_shape=jax.ShapeDtypeStruct((count, chips * lanes), jnp.bfloat16),
        in_specs=[whole()] * 3,
        out_specs=whole(),
        scratch_shapes=slots + [tile, tile] + sems + [pltpu.SemaphoreType.DMA((chips,))] * 2,
        compiler_params=remote_params(number),
        name="project",
    )(a, b, weight)


def gather_rows(chips, number, rows, notes, gate_w, up_w):
    count, width = rows.shape
    a = jnp.concatenate([rows[:, : width // 2], notes], axis=1)
    b = rows[:, width // 2 :]
    slots, sems = spread_scratch(chips, a, b)
    return pl.pallas_call(
        functools.partial(gather_kernel, chips),
        out_shape=(
            jax.ShapeDtypeStruct((chips * count, width), jnp.bfloat16),
            jax.ShapeDtypeStruct((chips * count, LANES), jnp.bfloat16),
            jax.ShapeDtypeStruct((chips * count, gate_w.shape[1]), jnp.bfloat16),
        ),
        in_specs=[whole()] * 4,
        out_specs=(whole(),) * 3,
        scratch_shapes=slots + sems,
        compiler_params=remote_params(number),
        name="gather_rows",
    )(a, b, gate_w, up_w)


def down_project(chips, number, hidden, gain, weight):
    count, lanes = hidden.shape
    a, b = hidden[: count // 2], hidden[count // 2 :]
    slots, sems = spread_scratch(chips, a, b)
    tile = pltpu.VMEM((chips, count // chips, lanes), jnp.bfloat16)
    return pl.pallas_call(
        functools.partial(down_kernel, chips),
        out_shape=jax.ShapeDtypeStruct((count // chips, chips * lanes), jnp.bfloat16),
        in_specs=[whole()] * 4,
        out_specs=whole(),
        scratch_shapes=slots + [tile, tile] + sems + [pltpu.SemaphoreType.DMA((chips,))] * 2,
        compiler_params=remote_params(number),
        name="down_project",
    )(a, b, gain[None, :], weight)


def stick_kernel(lens_ref, q_ref, k_ref, v_ref, bias_ref, out_ref):
    step = pl.program_id(0)
    batch, span, _ = k_ref.shape
    blocks = span // LANES
    row = lax.broadcasted_iota(jnp.int32, (3 * LANES, LANES), 0)
    column = lax.broadcasted_iota(jnp.int32, (3 * LANES, LANES), 1)
    after = (lax.rem(row, LANES) > column).astype(jnp.bfloat16)
    place = lax.broadcasted_iota(jnp.int32, (HEADS, span), 1)
    bias = bias_ref[:, :1]
    group = HEADS // KV_HEADS
    head = lax.broadcasted_iota(jnp.int32, (HEADS, LANES), 0)
    lane = lax.broadcasted_iota(jnp.int32, (HEADS, LANES), 1)
    own_lanes = (head // group) == (lane // HEAD_DIM)
    late = lax.broadcasted_iota(jnp.int32, (HEADS, HEAD_DIM), 0) >= group
    for item in range(batch):
        heads = q_ref[item].astype(jnp.float32)
        heads = jnp.where(own_lanes, jnp.concatenate([heads] * KV_HEADS, axis=1), 0.0)
        scores = lax.dot_general(
            heads.astype(jnp.bfloat16), k_ref[item], (((1,), (1,)), ((), ())), preferred_element_type=jnp.float32
        )
        scores = scores * HEAD_DIM ** (-0.5) + bias
        live = place < lens_ref[step * batch + item]
        remain = -(jnp.maximum(scores, 0.0) + jnp.log1p(jnp.exp(-jnp.abs(scores))))
        log_remain = jnp.where(live, remain, 0.0)
        stacked = jnp.concatenate(
            [log_remain[:, n * LANES : (n + 1) * LANES] for n in range(blocks)], axis=0
        )
        high = stacked.astype(jnp.bfloat16)
        rest = stacked - high.astype(jnp.float32)
        middle = rest.astype(jnp.bfloat16)
        low = (rest - middle.astype(jnp.float32)).astype(jnp.bfloat16)
        within = jnp.dot(
            jnp.concatenate([high, middle, low], axis=1), after, preferred_element_type=jnp.float32
        )
        totals = jnp.sum(stacked, axis=1, keepdims=True)
        carried = jnp.zeros((HEADS, 1), jnp.float32)
        pieces = [None] * blocks
        for n in range(blocks - 1, -1, -1):
            pieces[n] = within[n * HEADS : (n + 1) * HEADS] + carried
            carried = carried + totals[n * HEADS : (n + 1) * HEADS]
        remain_after = jnp.concatenate(pieces, axis=1)
        weights = jnp.where(live, jnp.exp(scores + remain + remain_after), 0.0)
        mixed = jnp.dot(
            weights.astype(jnp.bfloat16), v_ref[item], preferred_element_type=jnp.float32
        )
        mixed = jnp.where(late, mixed[:, HEAD_DIM:], mixed[:, :HEAD_DIM])
        out_ref[item] = mixed.astype(jnp.bfloat16)


def stick_read(queries, key_cache, value_cache, lengths, head_bias):
    batch, span, lanes = key_cache.shape
    heads = queries.reshape(batch, HEADS, HEAD_DIM)
    each = min(4, batch)
    mixed = pl.pallas_call(
        stick_kernel,
        out_shape=jax.ShapeDtypeStruct((batch, HEADS, HEAD_DIM), jnp.bfloat16),
        grid=(batch // each,),
        in_specs=[
            pl.BlockSpec(memory_space=pltpu.SMEM),
            pl.BlockSpec((each, HEADS, HEAD_DIM), lambda i: (i, 0, 0)),
            pl.BlockSpec((each, span, lanes), lambda i: (i, 0, 0)),
            pl.BlockSpec((each, span, lanes), lambda i: (i, 0, 0)),
            pl.BlockSpec((HEADS, LANES), lambda i: (0, 0)),
        ],
        out_specs=pl.BlockSpec((each, HEADS, HEAD_DIM), lambda i: (i, 0, 0)),
        name="stick_read",
    )(lengths, heads, key_cache, value_cache, jnp.broadcast_to(head_bias[:, None], (HEADS, LANES)))
    return mixed.reshape(batch, HEADS * HEAD_DIM)


def shards(
    tokens,
    cache_keys,
    cache_values,
    cache_len,
    norm_gain_first,
    w_query,
    w_key,
    w_value,
    head_bias,
    w_output,
    norm_gain_second,
    group_id,
    member,
    group_gate,
    member_weight,
    expert_gate_w,
    expert_up_w,
    expert_down_w,
    dense_gate_w,
    dense_up_w,
    hidden_gain,
    dense_down_w,
    branch_logit,
):
    devices = lax.axis_size("ep")
    chips = devices // 2
    me = lax.axis_index("ep")
    first = lax.rem(me, 2) == 0
    partner = [(i, i + 1 - 2 * (i % 2)) for i in range(devices)]
    seq_dev, width = tokens.shape

    def both(own):
        other = lax.ppermute(own, "ep", partner)
        return jnp.where(
            first, jnp.concatenate([own, other], axis=-1), jnp.concatenate([other, own], axis=-1)
        )

    query_w = both(w_query)
    output_w = both(w_output)
    gate_w = both(dense_gate_w)
    up_w = both(dense_up_w)
    down_w = both(dense_down_w)

    stream = tokens.astype(jnp.float32)
    normed_first = (stream * rms_scale(stream) * norm_gain_first).astype(jnp.bfloat16)
    new_keys = jnp.dot(normed_first, w_key, preferred_element_type=jnp.float32).astype(jnp.bfloat16)
    new_values = jnp.dot(normed_first, w_value, preferred_element_type=jnp.float32).astype(
        jnp.bfloat16
    )
    queries = project(chips, 1, normed_first, query_w)
    attended = stick_read(queries, cache_keys, cache_values, cache_len, head_bias)
    projected = project(chips, 2, attended, output_w)
    second_stream = stream + projected.astype(jnp.float32)
    normed_second = (second_stream * rms_scale(second_stream) * norm_gain_second).astype(
        jnp.bfloat16
    )

    experts = devices * expert_gate_w.shape[0]
    capacity = seq_dev // (experts // PER_GROUP)
    notes = jnp.concatenate(
        [member, group_id[:, None], jnp.zeros((seq_dev, LANES - TOP_K - 1), jnp.int32)], axis=1
    ).astype(jnp.bfloat16)
    own_rows, own_notes, hidden = gather_rows(chips, 3, normed_second, notes, gate_w, up_w)
    other_rows = lax.ppermute(own_rows, "ep", partner)
    other_notes = lax.ppermute(own_notes, "ep", partner)
    dense_out = down_project(chips, 4, hidden, hidden_gain, down_w)

    def selection(rows_notes, parity):
        table = rows_notes[:, : TOP_K + 1].astype(jnp.int32)
        named = table[:, TOP_K :] * PER_GROUP + table[:, :TOP_K]
        hits = jnp.any(named == me, axis=1).reshape(chips, seq_dev)
        index = jnp.arange(seq_dev)
        earlier = (index[:, None] < index[None, :]).astype(jnp.float32)
        slot = jnp.dot(hits.astype(jnp.float32), earlier).astype(jnp.int32)
        spot = ((jnp.arange(chips)[:, None] * 2 + parity) * capacity + slot).reshape(-1)
        spot = jnp.where(hits.reshape(-1), spot, -1)
        return (jnp.arange(devices * capacity)[:, None] == spot[None, :]).astype(jnp.bfloat16)

    parity = lax.rem(me, 2)
    packed = jnp.dot(selection(own_notes, parity), own_rows, preferred_element_type=jnp.float32)
    packed = packed + jnp.dot(
        selection(other_notes, 1 - parity), other_rows, preferred_element_type=jnp.float32
    )
    packed = packed.astype(jnp.bfloat16)
    gate_pre = jnp.dot(packed, expert_gate_w[0], preferred_element_type=jnp.float32)
    upper_pre = jnp.dot(packed, expert_up_w[0], preferred_element_type=jnp.float32)
    expert_hidden = (jax.nn.silu(gate_pre) * upper_pre).astype(jnp.bfloat16)
    served = jnp.dot(expert_hidden, expert_down_w[0], preferred_element_type=jnp.float32).astype(
        jnp.bfloat16
    )
    returned = lax.all_to_all(
        served.reshape(devices, capacity, width), "ep", split_axis=0, concat_axis=0, tiled=True
    ).reshape(experts * capacity, width)

    pair_expert = (group_id[:, None] * PER_GROUP + member).reshape(-1)
    pair_count = pair_expert.shape[0]
    expert_hits = (pair_expert[:, None] == jnp.arange(experts, dtype=jnp.int32)[None, :]).astype(
        jnp.float32
    )
    earlier = (jnp.arange(pair_count)[:, None] > jnp.arange(pair_count)[None, :]).astype(
        jnp.float32
    )
    before = jnp.dot(earlier, expert_hits, preferred_element_type=jnp.float32)
    slot_index = jnp.sum(before * expert_hits, axis=1).astype(jnp.int32)
    target = pair_expert * capacity + slot_index
    select = (target[:, None] == jnp.arange(experts * capacity, dtype=jnp.int32)[None, :]).astype(
        jnp.bfloat16
    )
    pair_out = jnp.dot(select, returned, preferred_element_type=jnp.float32)
    combine = (group_gate[:, None] * member_weight).reshape(-1, 1)
    routed = jnp.sum((pair_out * combine).reshape(seq_dev, TOP_K, width), axis=1)
    mixed_out = (
        second_stream + routed + jax.nn.sigmoid(branch_logit) * dense_out.astype(jnp.float32)
    )
    return (mixed_out.astype(jnp.bfloat16), new_keys, new_values)


LOG2E = 1.4426950408889634
DEAD = -1e30
BATCHES = 2
TRANSPOSED = (((1,), (1,)), ((), ()))
ORDERS = (("x", "y"), ("y", "x"))


def dot_t(a, b):
    return lax.dot_general(a, b, TRANSPOSED, preferred_element_type=jnp.float32)


def dot(a, b):
    return jnp.dot(a, b, preferred_element_type=jnp.float32)


def remote(src, dst, send, recv, device):
    return pltpu.make_async_remote_copy(
        src_ref=src, dst_ref=dst, send_sem=send, recv_sem=recv, device_id=device, device_id_type=MESH
    )


class Grid(Place):
    def __init__(self, chips):
        super().__init__(chips)
        self.partner = (self.chip * 2 + 1 - self.core,)
        self.depth = self.dims[0]
        self.plane = chips // self.depth

    def on(self, z, dy=0, dx=0):
        depth, height, width = self.dims
        y = lax.rem(self.y + dy, height)
        x = lax.rem(self.x + dx, width)
        return (z * height + y) * width + x

    def turn(self, axis):
        return (1, 0) if axis == "y" else (0, 1)

    def sweep(self, step):
        toward = 1 - 2 * (self.z // (self.depth // 2))
        return lax.rem(self.z + step * toward + self.depth, self.depth)

    def enter(self):
        barrier = pltpu.get_barrier_semaphore()
        for step in range(1, self.chips):
            other = lax.rem(self.chip + step, self.chips)
            pl.semaphore_signal(barrier, inc=1, device_id=self.device(other), device_id_type=MESH)
        pl.semaphore_signal(barrier, inc=1, device_id=self.partner, device_id_type=MESH)
        pl.semaphore_wait(barrier, self.chips)


class Clock:
    def __init__(self):
        self.now = 0.0

    def spend(self, time):
        self.now += time

    def run(self, batches):
        ready = {batch: 0.0 for batch in batches}
        while ready:
            batch = min(ready, key=lambda b: (max(ready[b], self.now), batches.index(b)))
            self.now = max(self.now, ready[batch])
            following = next(batch, None)
            if following is None:
                del ready[batch]
            else:
                ready[batch] = following


class Gather:
    def __init__(self, place, clock, send, recv, groups, pieces):
        self.place = place
        self.clock = clock
        self.send = send
        self.recv = recv
        self.groups = groups
        self.pieces = pieces

    def copy(self, piece, origin, index, target):
        view = self.pieces[piece](origin)
        return remote(view, view, self.send.at[piece], self.recv.at[piece, index], self.place.device(target))

    def several(self, piece, count, index):
        view = self.pieces[piece](pl.ds(0, count))
        return remote(view, view, self.send.at[piece], self.recv.at[piece, index],
                      self.place.device(self.place.chip))

    def turns(self, piece):
        first, second = ORDERS[piece]
        return self.place.turn(first), self.place.turn(second)

    def last(self, step):
        return 2 * self.place.depth + step * self.groups // self.place.depth

    def across(self, piece, step):
        place = self.place
        first, second = self.turns(piece)
        z = place.sweep(step)
        self.copy(piece, place.on(z), place.depth + z, place.on(place.z, *first)).start()
        self.copy(piece, place.on(z), self.last(step), place.on(place.z, *second)).start()

    def corner(self, piece, step):
        place = self.place
        first, second = self.turns(piece)
        z = place.sweep(step)
        origin = place.on(z, *first)
        self.copy(piece, origin, place.depth + z, place.chip).wait_recv()
        self.copy(piece, origin, self.last(step), place.on(place.z, *second)).start()

    def steps(self):
        place, depth = self.place, self.place.depth
        every = range(len(self.pieces))
        begin = self.begin = self.clock.now
        for step in range(1, depth):
            for piece in every:
                self.copy(piece, place.chip, place.z, place.on(place.sweep(step))).start()
        for piece in every:
            self.across(piece, 0)
        self.clock.spend(0.1)
        yield begin + 3.0
        for piece in every:
            self.corner(piece, 0)
        for step in range(1, depth):
            yield begin + 2.6 + 1.1 * step
            for piece in every:
                z = place.sweep(step)
                self.copy(piece, place.on(z), z, place.chip).wait_recv()
                self.across(piece, step)
        for step in range(1, depth):
            yield begin + 5.0 + 1.1 * step
            for piece in every:
                self.corner(piece, step)

    def rest(self, group):
        for piece in range(len(self.pieces)):
            self.several(piece, 2 * self.place.depth // self.groups, 2 * self.place.depth + group).wait_recv()

    def due(self, group):
        return self.begin + 7.5 + 1.1 * ((group + 1) * self.place.depth // self.groups - 1)

    def finish(self):
        for piece in range(len(self.pieces)):
            self.several(piece, self.place.chips - 1, 0).wait_send()


def norm_rows(values, gain):
    square = jnp.mean(values * values, axis=-1, keepdims=True)
    return (values * lax.rsqrt(square + epsilon) * gain).astype(jnp.bfloat16)


def layer_kernel(
    chips, names,
    lens_ref, ids_ref, bias_ref, tokens_ref, gain1_ref, gain2_ref, hgain_ref, logit_ref,
    member_ref, mweight_ref, group_ref, ggate_ref,
    keys_hbm, values_hbm, wq_hbm, wo_hbm, wg_hbm, wu_hbm, wd_hbm, wk_hbm, wv_hbm, eg_hbm, eu_hbm, ed_hbm,
    out_ref, newk_ref, newv_ref,
    *scratch,
):
    s = types.SimpleNamespace(**dict(zip(names, scratch)))
    place = Grid(chips)
    clock = Clock()
    me = place.chip * 2 + place.core
    chip, core, z, depth, plane = place.chip, place.core, place.z, place.depth, place.plane
    tokens, width = tokens_ref.shape
    seq = tokens // BATCHES
    half = width // 2
    rows = chips * seq
    lanes = LANES
    experts = chips * 2
    part = plane * seq
    bf16, f32 = jnp.bfloat16, jnp.float32
    cut = lanes + half
    chunk = width // 4
    group = me // PER_GROUP

    own_rows = pl.ds(pl.multiple_of(core * (lanes // 2), lanes // 2), lanes // 2)
    spot_me = lax.rem(chip, plane)
    weights = (
        (s.wq.at[own_rows], wq_hbm), (s.wo.at[spot_me, core], wo_hbm),
        (s.wg.at[own_rows], wg_hbm), (s.wu.at[own_rows], wu_hbm),
    )
    waiting = {}

    def fetch(key, src, dst):
        copy = pltpu.make_async_copy(src, dst, s.local_sem.at[len([k for k in waiting if k < 20])])
        copy.start()
        waiting[key] = copy.wait

    ended = set()

    def need(*keys):
        for key in keys:
            if key not in ended:
                ended.add(key)
                waiting[key]()

    for i, (dst, src) in enumerate(weights):
        fetch(i, src, dst)
    fetch(4, wk_hbm, s.wk)
    fetch(5, wv_hbm, s.wv)
    fetch(6, keys_hbm, s.keys)
    fetch(7, values_hbm, s.values)
    fetch(8, eg_hbm.at[0], s.eg)
    fetch(9, eu_hbm.at[0], s.eu)
    fetch(10, ed_hbm.at[0], s.ed)

    place_of = lax.broadcasted_iota(jnp.int32, (lanes, tokens), 0)
    expert = lax.rem(place_of, experts)
    combine = jnp.zeros((lanes, tokens), f32)
    for k in range(TOP_K):
        named = group_ref[...] * PER_GROUP + member_ref[k : k + 1, :]
        weight = ggate_ref[...] * mweight_ref[k : k + 1, :]
        combine = jnp.where(expert == named, weight, combine)
    high = combine.astype(bf16).astype(f32)
    notes = jnp.where(place_of < experts, high, jnp.where(place_of < 2 * experts, combine - high, 0.0))
    square = (tokens, tokens)
    row, column = (lax.broadcasted_iota(jnp.int32, square, axis) for axis in (0, 1))
    forward = backward = jnp.zeros(square, f32)
    order = [0] * tokens
    later = 0
    for token in range(tokens):
        named = ids_ref[token]
        slot = named * (seq + later) + (1 - named) * (token - later)
        later = later + named
        forward = jnp.where((row == slot) & (column == token), 1.0, forward)
        backward = jnp.where((row == token) & (column == slot), 1.0, backward)
        order = [jnp.where(slot == k, token, order[k]) for k in range(tokens)]
    forward, backward = forward.astype(bf16), backward.astype(bf16)
    notes = dot_t(forward, notes.astype(bf16)).astype(bf16)
    sorted_tokens = dot(forward, tokens_ref[...]).astype(bf16)
    for b in range(BATCHES):
        s.slots1[b, chip, :, :lanes] = notes[b * seq : (b + 1) * seq]
        s.slots1[b, chip, :, lanes:] = sorted_tokens[b * seq : (b + 1) * seq]

    span = s.keys.shape[1]
    blocks = span // lanes
    row = lax.broadcasted_iota(jnp.int32, (2 * lanes, 2 * lanes), 0)
    column = lax.broadcasted_iota(jnp.int32, (2 * lanes, 2 * lanes), 1)
    s.after[...] = jnp.where((lax.rem(row, lanes) > column) | (column >= lanes), 1.0, 0.0).astype(bf16)
    head_row = lax.broadcasted_iota(jnp.int32, (HEADS, lanes), 0)
    bias = jnp.zeros((HEADS, lanes), f32)
    for head in range(HEADS):
        bias = jnp.where(head_row == (head % 2) * chips + head // 2, bias_ref[head] * LOG2E, bias)
    s.bias[...] = bias

    place.enter()

    swaps = [
        remote(src, dst, s.swap_send.at[i], s.swap_recv.at[i], place.partner)
        for i, (dst, src) in enumerate(weights)
    ]
    for i, swap in enumerate(swaps):
        waiting[20 + i] = swap.wait_recv

    def down_copy(target):
        columns = pl.ds(pl.multiple_of(target * lanes, lanes), lanes)
        return remote(wd_hbm.at[:, columns], s.wd.at[chip, core], s.down_send.at[0],
                      s.down_recv.at[0], place.device(target))

    peers = ((0, 1), (1, 0), (1, 1))

    def wide_copy(index, target):
        return remote(wo_hbm, s.wo.at[spot_me, core], s.wide_send.at[0], s.wide_recv.at[index], place.device(target))

    def wide_pass(index):
        view = s.wo.at[lax.rem(place.on(z, *peers[index]), plane), core]
        arrived(view, s.wide_recv.at[index])
        remote(view, view, s.pass_send.at[0], s.pass_recv.at[0], place.partner).start()

    def spot(of):
        return lax.rem(of, plane) * depth + of // plane

    down_swap = remote(s.wd.at[:, core], s.wd.at[:, core], s.swap_send.at[4], s.swap_recv.at[4], place.partner)
    waiting[24] = down_swap.wait_recv

    def arrived(view, recv):
        remote(view, view, s.down_send.at[0], recv, place.device(chip)).wait_recv()

    def departed(view, send):
        return remote(view, view, send, s.down_recv.at[0], place.device(chip)).wait_send

    def others():
        return [lax.rem(chip + step, chips) for step in range(1, chips)]

    others_ds = pl.ds(0, chips - 1)

    def attend(b, item):
        jrow = lax.broadcasted_iota(jnp.int32, (chips, lanes), 0)
        jlane = lax.broadcasted_iota(jnp.int32, (chips, lanes), 1)
        early = jrow < chips // KV_HEADS
        own = (jlane // HEAD_DIM) == (jrow // (chips // KV_HEADS))
        even = s.heads[b, item]
        turned = pltpu.roll(even, HEAD_DIM, axis=1)
        query = jnp.concatenate([
            jnp.where(own, jnp.where(early, even, turned), 0.0),
            jnp.where(own, jnp.where(early, turned, even), 0.0),
        ], axis=0).astype(bf16)
        index = order[b * seq + item]
        scores = dot_t(query, s.keys[index]) * (HEAD_DIM ** (-0.5) * LOG2E)
        scores = scores + jnp.concatenate([s.bias[...]] * blocks, axis=1)
        position = lax.broadcasted_iota(jnp.int32, (HEADS, span), 1)
        scores = jnp.where(position < lens_ref[index], scores, DEAD)
        soft = jnp.maximum(scores, 0.0) + jnp.log(1.0 + jnp.exp2(-jnp.abs(scores))) * LOG2E
        stacked = jnp.concatenate([soft[:, n * lanes : (n + 1) * lanes] for n in range(blocks)], axis=0)
        top = stacked.astype(bf16)
        low = (stacked - top.astype(f32)).astype(bf16)
        sums = dot(jnp.concatenate([top, low], axis=1), s.after[...])
        carried = jnp.zeros((HEADS, lanes), f32)
        pieces = [None] * blocks
        for n in range(blocks - 1, -1, -1):
            band = sums[n * HEADS : (n + 1) * HEADS]
            spent = stacked[n * HEADS : (n + 1) * HEADS] + band[:, :lanes] + carried
            pieces[n] = jnp.exp2(scores[:, n * lanes : (n + 1) * lanes] - spent).astype(bf16)
            carried = carried + band[:, lanes:]
        found = dot(jnp.concatenate(pieces, axis=1), s.values[index])
        first, second = found[:chips], found[chips:]
        s.mixed[b, item] = jnp.where(
            jlane < HEAD_DIM,
            jnp.where(early, first, pltpu.roll(first, HEAD_DIM, axis=1)),
            jnp.where(early, pltpu.roll(second, HEAD_DIM, axis=1), second),
        )

    def columns_of(piece):
        return slice(piece * half, (piece + 1) * half)

    sends = []

    def batch(b):
        slots1, slots2, slots3 = s.slots1.at[b], s.slots2.at[b], s.slots3.at[b]
        gather = Gather(place, clock, s.gather_send.at[b, 0], s.gather_recv.at[b, 0], depth // 2, (
            lambda o: slots1.at[o, :, pl.ds(0, cut)],
            lambda o: slots1.at[o, :, pl.ds(cut, half)],
        ))
        sends.append(gather.finish)
        steps = gather.steps()
        yield next(steps)
        if b == 0:
            for swap in swaps:
                swap.start()
                sends.append(swap.wait_send)
        yield from steps

        tiles, landed = s.tiles.at[b], s.landed.at[b]

        def tile_copy(target):
            return remote(tiles.at[target], landed.at[chip], s.tile_send.at[b], s.tile_recv.at[b],
                          place.device(target))

        for pair in range(depth // 2):
            yield gather.due(pair)
            need(0, 20)
            gather.rest(pair)
            planes = []
            for step in (2 * pair, 2 * pair + 1):
                zo = place.sweep(step)
                planes.append(slots1[pl.ds(zo * plane, plane), :, lanes:].reshape(part, width))
            normed = norm_rows(jnp.concatenate(planes, axis=0).astype(f32), gain1_ref[...])
            product = dot_t(normed, s.wq[...]).astype(bf16).reshape(2, plane, seq, lanes)
            for side, step in enumerate((2 * pair, 2 * pair + 1)):
                zo = place.sweep(step)
                tiles[pl.ds(zo * plane, plane)] = product[side]
                for dy in (1, 0):
                    for dx in (1, 0):
                        if (step, dy, dx) != (0, 0, 0):
                            tile_copy(place.on(zo, dy, dx)).start()
            clock.spend(0.6)
        landed[chip] = tiles[chip]
        sends.append(departed(tiles.at[others_ds], s.tile_send.at[b]))
        begin = clock.now

        if b == BATCHES - 1:
            for index, turn in enumerate(peers):
                wide_copy(index, place.on(z, *turn)).start()
            for target in others():
                down_copy(target).start()
            sends.append(departed(s.wd.at[others_ds, core], s.down_send.at[0]))
            sends.append(departed(s.wo.at[pl.ds(0, 3), 0], s.wide_send.at[0]))
            sends.append(departed(s.wo.at[pl.ds(0, 3), 0], s.pass_send.at[0]))
            fetch(11, wd_hbm.at[:, pl.ds(pl.multiple_of(chip * lanes, lanes), lanes)], s.wd.at[chip, core])
            need(4, 5)
            own_normed = norm_rows(tokens_ref[...].astype(f32), gain1_ref[...])
            newk_ref[...] = dot(own_normed, s.wk[...]).astype(bf16)
            newv_ref[...] = dot(own_normed, s.wv[...]).astype(bf16)
            clock.spend(0.4)
        yield begin + 4.0
        arrived(landed.at[others_ds], s.tile_recv.at[b])
        for j in range(chips):
            s.heads[b, :, j, :] = landed[j].astype(f32)
        need(6, 7)
        for item in range(seq):
            attend(b, item)
            if item % 2 == 1:
                clock.spend(0.9)
                yield clock.now
        for j in range(chips):
            slots2[z, :, j * lanes : (j + 1) * lanes] = s.mixed[b, :, j, :].astype(bf16)
        clock.spend(0.1)

        begin = clock.now
        for step in range(depth - 1, 0, -1):
            remote(slots2.at[z], slots2.at[z], s.line_send.at[b], s.line_recv.at[b],
                   place.device(place.on(place.sweep(step)))).start()
        line_view = slots2.at[pl.ds(0, depth - 1)]
        sends.append(departed(line_view, s.line_send.at[b]))
        if b == 0:
            for index in range(3):
                yield begin + 0.9 + 0.9 * index
                if index == 0:
                    need(1)
                wide_pass(index)
        yield begin + 5.5
        arrived(line_view, s.line_recv.at[b])
        need(21)
        if b == 0:
            arrived(s.wo.at[pl.ds(0, 3), 0], s.pass_recv.at[0])
        line_rows = slots2[...].reshape(depth * seq, width)
        product = dot_t(line_rows, s.wo[...].reshape(plane * lanes, width)).astype(bf16)
        slots3[chip] = product.reshape(depth, seq, plane * lanes)
        clock.spend(0.7)

        gather = Gather(place, clock, s.gather_send.at[b, 1], s.gather_recv.at[b, 0], 1, (
            lambda o: slots3.at[o, pl.ds(0, depth // 2)],
            lambda o: slots3.at[o, pl.ds(depth // 2, depth // 2)],
        ))
        sends.append(gather.finish)
        yield from gather.steps()
        if b == 0:
            need(11)
            arrived(s.wd.at[others_ds, core], s.down_recv.at[0])
            down_swap.start()
            sends.append(down_swap.wait_send)
        both = s.rows.at[b]
        acc = s.acc.at[b]

        def serve(c, lent):
            if lent:
                arrived(both.at[c], s.row_recv.at[b])
            every = both[c, :, :width]
            served = (jax.nn.silu(dot(every, s.eg[...])) * dot(every, s.eu[...])).astype(bf16)
            note_lane = lax.broadcasted_iota(jnp.int32, (rows, lanes), 1)
            mine = (note_lane == me) | (note_lane == me + experts)
            weight = jnp.sum(jnp.where(mine, both[c, :, width:].astype(f32), 0.0), axis=1, keepdims=True)
            for n in range(4):
                at = slice(n * chunk, (n + 1) * chunk)
                value = dot(served, s.ed[:, at])
                value = jnp.where(weight != 0.0, value * weight, 0.0)
                if lent:
                    s.gift[n] = value.astype(bf16)
                    remote(s.gift.at[n], s.given.at[n], s.gift_send.at[0], s.gift_recv.at[n // 2],
                           place.partner).start()
                else:
                    acc[:, :, at] = value.reshape(chips, seq, chunk)

        yield gather.due(0)
        need(8, 9, 10)

        if b == 0:

            @pl.when((group == b) & (core == 0))
            def _():
                serve(1, True)

            clock.spend(0.6)
        gather.rest(0)

        block = rows // 2
        served_here = pl.when(group == b)
        line = depth * seq
        for n in range(2):
            at = slice(n * block, (n + 1) * block)
            for p in range(n * plane // 2, (n + 1) * plane // 2):
                of = slice(p * line, (p + 1) * line)
                token = jnp.concatenate(
                    [slots1[k * plane + p, :, lanes:].astype(f32) for k in range(depth)], axis=0)
                projected = jnp.concatenate(
                    [slots3[k * plane + p].reshape(line, plane * lanes) for k in range(depth)], axis=1)
                both[core, of, :width] = norm_rows(token + projected.astype(f32), gain2_ref[...])
                for k in range(depth):
                    both[core, p * line + k * seq : p * line + (k + 1) * seq, width:] = (
                        slots1[k * plane + p, :, :lanes])

            @served_here
            def _():
                remote(both.at[core, at], both.at[core, at], s.row_send.at[b], s.row_recv.at[b],
                       place.partner).start()

        clock.spend(0.4)

        need(2, 3, 22, 23)
        normed = both[core, :, :width]
        gate = dot_t(normed, s.wg[...])
        hidden = jax.nn.silu(gate) * dot_t(normed, s.wu[...])
        s.hidden[b] = hidden
        squares = s.squares.at[b]
        summed = jnp.broadcast_to(jnp.sum(hidden * hidden, axis=1, keepdims=True), (rows, lanes))
        squares[chip] = jnp.transpose(summed)[:1]

        def square_copy(target):
            return remote(squares.at[chip], squares.at[chip], s.square_send.at[b],
                          s.square_recv.at[b], place.device(target))

        for target in others():
            square_copy(target).start()
        sends.append(departed(squares.at[others_ds], s.square_send.at[b]))
        clock.spend(0.5)
        sent_at = clock.now

        for c in range(2):

            @pl.when((group == b) & (core == c))
            def _():
                serve(c, False)

        clock.spend(1.0)
        yield sent_at + 5.5

        @pl.when((group == b) & (core == 1))
        def _():
            serve(0, True)

        if b > 0:

            @pl.when((group == b) & (core == 0))
            def _():
                serve(1, True)

        clock.spend(0.6)

        def end_served():
            @pl.when(group == b)
            def _():
                departed(both.at[core], s.row_send.at[b])()
                departed(s.gift, s.gift_send.at[0])()

        sends.append(end_served)

        arrived(squares.at[others_ds], s.square_recv.at[b])
        total = squares[0]
        for c in range(1, chips):
            total = total + squares[c]
        scale = lax.rsqrt(total / width + epsilon)
        scale = jnp.transpose(jnp.broadcast_to(scale, (lanes, rows)))
        gain = hgain_ref[:, pl.ds(pl.multiple_of(chip * lanes, lanes), lanes)]
        dense = (s.hidden[b] * scale * gain).astype(bf16)
        need(24)

        stage = s.stage.at[b]

        def staged(piece, value, slot, index, recv, target):
            stage[piece, slot] = value.astype(bf16)
            remote(stage.at[piece, slot], s.sums.at[b, piece, index], s.sum_send.at[b, piece],
                   s.sum_recv.at[b, piece, recv], place.device(target)).start()

        def summands(piece, index, count, recv):
            view = s.sums.at[b, piece, pl.ds(index, count)]
            arrived(view, s.sum_recv.at[b, piece, recv])

        def summand(piece, index):
            return s.sums[b, piece, index].astype(f32)

        for piece in range(2):
            sends.append(departed(stage.at[piece, pl.ds(0, 4 * depth - 1)], s.sum_send.at[b, piece]))
            first, second = (place.turn(a) for a in ORDERS[piece])

            @served_here
            def _():
                arrived(s.given.at[pl.ds(2 * piece, 2)], s.gift_recv.at[piece])

            for c in (2 * piece, 2 * piece + 1):
                at = slice(c * chunk, (c + 1) * chunk)
                down = s.wd[c * (chips // 4) : (c + 1) * (chips // 4)].reshape(chunk, lanes)
                value = jax.nn.sigmoid(logit_ref[:, at]) * dot_t(dense, down)
                value = value.reshape(chips, seq, chunk)

                @served_here
                def _():
                    acc[:, :, at] += s.given[c].astype(f32).reshape(chips, seq, chunk) + value

                @pl.when(group != b)
                def _():
                    acc[:, :, at] = value

            for beside in (1, 0):
                for step in range(depth - 1, -1, -1):
                    zo = place.sweep(step)
                    turn = (1, 1) if beside else first
                    index, recv = (zo, zo) if beside else (depth + 2 * zo, depth + zo)
                    staged(piece, acc[spot(place.on(zo, *turn)), :, columns_of(piece)], step * 2 + beside,
                           index, recv, place.on(z, *first))
        clock.spend(1.0)
        begin = clock.now

        for step in range(depth - 1, -1, -1):
            yield begin + 2.5 + 0.8 * (depth - 1 - step)
            for piece in range(2):
                first, second = (place.turn(a) for a in ORDERS[piece])
                zo = place.sweep(step)
                summands(piece, zo, 1, zo)
                value = acc[spot(place.on(zo, *second)), :, columns_of(piece)] + summand(piece, zo)
                staged(piece, value, 2 * depth + step, depth + 2 * zo + 1, depth + zo, place.on(z, *second))

        def folded(piece, zo):
            summands(piece, depth + 2 * zo, 2, depth + zo)
            value = acc[spot(place.on(zo)), :, columns_of(piece)] + summand(piece, depth + 2 * zo)
            return value + summand(piece, depth + 2 * zo + 1)

        for step in range(depth - 1, 0, -1):
            yield begin + 5.2 + 0.8 * (depth - 1 - step)
            for piece in range(2):
                zo = place.sweep(step)
                staged(piece, folded(piece, zo), 3 * depth + step - 1, 3 * depth + z, 2 * depth, place.on(zo))
        yield begin + 8.0
        for piece in range(2):
            at = columns_of(piece)
            value = slots1[chip, :, lanes + piece * half : lanes + (piece + 1) * half].astype(f32)
            value = value + jnp.concatenate(
                [slots3[k * plane + spot_me, z] for k in range(piece * depth // 2, (piece + 1) * depth // 2)], axis=1
            ).astype(f32)
            acc[spot(chip), :, at] = value + folded(piece, z)
        yield begin + 11.0
        for piece in range(2):
            summands(piece, 3 * depth, depth - 1, 2 * depth)
            value = acc[spot(chip), :, columns_of(piece)]
            for step in range(1, depth):
                value = value + summand(piece, 3 * depth + place.sweep(step))
            s.final[b * seq : (b + 1) * seq, columns_of(piece)] = value.astype(bf16)

    clock.run([batch(b) for b in range(BATCHES)])
    out_ref[...] = dot(backward, s.final[...]).astype(bf16)
    for end in sends:
        end()


def copy_kernel(a_ref, b_ref, c_ref, a_out, b_out, c_out):
    a_out[...] = a_ref[...]
    b_out[...] = b_ref[...]
    c_out[...] = c_ref[...]


def layer_scratch(chips, depth, tokens, width, span, fe):
    n = BATCHES
    seq = tokens // n
    rows = chips * seq
    bf16, f32, DMA = jnp.bfloat16, jnp.float32, pltpu.SemaphoreType.DMA
    half = width // 2
    return dict(
        slots1=pltpu.VMEM((n, chips, seq, LANES + width), bf16),
        slots2=pltpu.VMEM((n, depth, seq, width), bf16),
        slots3=pltpu.VMEM((n, chips, depth, seq, chips // depth * LANES), bf16),
        keys=pltpu.VMEM((tokens, span, LANES), bf16),
        values=pltpu.VMEM((tokens, span, LANES), bf16),
        wq=pltpu.VMEM((LANES, width), bf16),
        wo=pltpu.VMEM((chips // depth, 2, LANES // 2, width), bf16),
        wg=pltpu.VMEM((LANES, width), bf16),
        wu=pltpu.VMEM((LANES, width), bf16),
        wk=pltpu.VMEM((width, LANES), bf16),
        wv=pltpu.VMEM((width, LANES), bf16),
        eg=pltpu.VMEM((width, fe), bf16),
        eu=pltpu.VMEM((width, fe), bf16),
        ed=pltpu.VMEM((fe, width), bf16),
        wd=pltpu.VMEM((chips, 2, LANES // 2, LANES), bf16),
        after=pltpu.VMEM((2 * LANES, 2 * LANES), bf16),
        bias=pltpu.VMEM((HEADS, LANES), f32),
        tiles=pltpu.VMEM((n, chips, seq, LANES), bf16),
        landed=pltpu.VMEM((n, chips, seq, LANES), bf16),
        heads=pltpu.VMEM((n, seq, chips, LANES), f32),
        mixed=pltpu.VMEM((n, seq, chips, LANES), f32),
        rows=pltpu.VMEM((n, 2, rows, width + LANES), bf16),
        final=pltpu.VMEM((tokens, width), bf16),
        hidden=pltpu.VMEM((n, rows, LANES), f32),
        squares=pltpu.VMEM((n, chips, 1, rows), f32),
        gift=pltpu.VMEM((4, rows, width // 4), bf16),
        given=pltpu.VMEM((4, rows, width // 4), bf16),
        acc=pltpu.VMEM((n, chips, seq, width), f32),
        stage=pltpu.VMEM((n, 2, 4 * depth, seq, half), bf16),
        sums=pltpu.VMEM((n, 2, 4 * depth, seq, half), bf16),
        local_sem=DMA((12,)),
        swap_send=DMA((5,)),
        swap_recv=DMA((5,)),
        gather_send=DMA((n, 2, 2)),
        gather_recv=DMA((n, 1, 2, 5 * depth // 2)),
        line_send=DMA((n,)),
        line_recv=DMA((n,)),
        wide_send=DMA((1,)),
        wide_recv=DMA((3,)),
        pass_send=DMA((1,)),
        pass_recv=DMA((1,)),
        tile_send=DMA((n,)),
        tile_recv=DMA((n,)),
        down_send=DMA((1,)),
        down_recv=DMA((1,)),
        square_send=DMA((n,)),
        square_recv=DMA((n,)),
        row_send=DMA((n,)),
        row_recv=DMA((n,)),
        gift_send=DMA((1,)),
        gift_recv=DMA((2,)),
        sum_send=DMA((n, 2)),
        sum_recv=DMA((n, 2, 2 * depth + 1)),
    )


def fused_shards(
    tokens, cache_keys, cache_values, cache_len, norm_gain_first, w_query, w_key, w_value, head_bias,
    w_output, norm_gain_second, group_id, member, group_gate, member_weight, expert_gate_w,
    expert_up_w, expert_down_w, dense_gate_w, dense_up_w, hidden_gain, dense_down_w, branch_logit,
):
    chips = lax.axis_size("ep") // 2
    seq, width = tokens.shape
    span = cache_keys.shape[1]
    bf16 = jnp.bfloat16
    scratch = layer_scratch(chips, torus_of(chips)[0], seq, width, span, expert_gate_w.shape[2])
    smem = pl.BlockSpec(memory_space=pltpu.SMEM)
    anywhere = pl.BlockSpec(memory_space=pl.ANY)
    out_shape = (
        jax.ShapeDtypeStruct((seq, width), bf16),
        jax.ShapeDtypeStruct((seq, LANES), bf16),
        jax.ShapeDtypeStruct((seq, LANES), bf16),
    )
    results = pl.pallas_call(
        functools.partial(layer_kernel, chips, tuple(scratch)),
        out_shape=out_shape,
        in_specs=[smem] * 3 + [whole()] * 9 + [anywhere] * 12,
        out_specs=(whole(),) * 3,
        scratch_shapes=list(scratch.values()),
        compiler_params=pltpu.CompilerParams(
            collective_id=1, has_side_effects=True, vmem_limit_bytes=60 * 1024 * 1024
        ),
        name="layer",
    )(
        cache_len, group_id, head_bias, tokens, norm_gain_first[None], norm_gain_second[None], hidden_gain[None],
        branch_logit[None], member.T, member_weight.T, group_id[None], group_gate[None],
        cache_keys, cache_values, w_query.T, w_output.T, dense_gate_w.T, dense_up_w.T, dense_down_w.T,
        w_key, w_value, expert_gate_w, expert_up_w, expert_down_w,
    )
    return pl.pallas_call(
        copy_kernel, out_shape=out_shape, in_specs=[whole()] * 3, out_specs=(whole(),) * 3, name="results"
    )(*results)


def one_kernel(mesh):
    chips = mesh.shape["ep"] // 2
    depth, height, width = torus_of(chips)
    return (height, width) == (2, 2) and chips * LANES == HEADS * HEAD_DIM and 4 * chips <= LANES and depth % 2 == 0 and 2 * chips == BATCHES * PER_GROUP


def solution(mesh):
    in_specs = (
        P("ep", None),
        P("ep", None, None),
        P("ep", None, None),
        P("ep"),
        P(),
        P(None, "ep"),
        P(),
        P(),
        P(),
        P(None, "ep"),
        P(),
        P("ep"),
        P("ep", None),
        P("ep"),
        P("ep", None),
        P("ep", None, None),
        P("ep", None, None),
        P("ep", None, None),
        P(None, "ep"),
        P(None, "ep"),
        P(),
        P(None, "ep"),
        P(),
    )
    out_specs = (P("ep", None), P("ep", None), P("ep", None))
    body = fused_shards if one_kernel(mesh) else shards
    return jax.shard_map(body, mesh=mesh, in_specs=in_specs, out_specs=out_specs, check_vma=False)
```

profile of v0, /device:TPU:0, one launch (start us, length us, event | category | flops | bytes accessed | tf_op | source)
XLA Modules:
  0.0 79.5 jit_solution(13999816970871617336)
XLA Ops:
  0.6 77.4 %layer.1 = (bf16[16,2048]{1,0:T(8,128)(2,1)}, bf16[16,128]{1,0:T(8,128)(2,1)}, bf16[16,128]{1,0:T(8,128)(2,1)}) custom-call(s32[16]{0:T(128)} %lens_ref.1, s32[16]{0:T(128)} %ids_ref.1, f32[32]{0:T(128)} %bias_ref.1, bf16[16,2048]{1,0:T(8,128)(2,1)} %tokens_ref.1, f32[1,2048]{1,0:T(1,128)} %bitcast.18, f32[1,2048]{1,0:T(1,128)} %bitcast.19, ...), custom_call_target="tpu_custom_call" | custom-call | tf_op jit(solution)/shard_map/layer/pallas_call | solution.py:1212
  78.0 1.5 %results.1 = (bf16[16,2048]{1,0:T(8,128)(2,1)}, bf16[16,128]{1,0:T(8,128)(2,1)}, bf16[16,128]{1,0:T(8,128)(2,1)}) custom-call(bf16[16,2048]{1,0:T(8,128)(2,1)} %get-tuple-element.6.a_ref, bf16[16,128]{1,0:T(8,128)(2,1)} %get-tuple-element.7.b_ref, bf16[16,128]{1,0:T(8,128)(2,1)} %get-tuple-element.8.c_ref), custom_call_target="tpu_custom_call" | custom-call | tf_op jit(solution)/shard_map/results/pallas_call | solution.py:1228
where the time goes:
time: 79.7 us; the launch traced here: 79.5 us
  Pallas kernels  78.9 us (99%)
    pallas_call x1, Pallas kernels, fused_shards(): pl.pallas_call(functools.partial(layer_kernel, chips, tuple(scratch)), ou...  77.4 us

commit v1 on v0

--- a/solution.py
+++ b/solution.py
@@ -744,10 +744,22 @@
     for i, swap in enumerate(swaps):
         waiting[20 + i] = swap.wait_recv
 
-    def down_copy(target):
-        columns = pl.ds(pl.multiple_of(target * lanes, lanes), lanes)
-        return remote(wd_hbm.at[:, columns], s.wd.at[chip, core], s.down_send.at[0],
-                      s.down_recv.at[0], place.device(target))
+    def down_line(zo):
+        columns = pl.ds(pl.multiple_of(zo * plane * lanes, plane * lanes), plane * lanes)
+        return wd_hbm.at[:, columns], s.transit.at[z]
+
+    def down_cut(position):
+        columns = pl.ds(pl.multiple_of(position * lanes, lanes), lanes)
+        return s.transit.at[:, :, columns], s.wd.at[:, spot_me, core]
+
+    def down_across():
+        need(11)
+        arrived(s.transit.at[pl.ds(0, depth - 1)], s.down_recv.at[0])
+        for turn in peers:
+            target = place.on(z, *turn)
+            remote(*down_cut(lax.rem(target, plane)), s.down_send.at[1], s.down_recv.at[1],
+                   place.device(target)).start()
+        fetch(12, *down_cut(spot_me))
 
     peers = ((0, 1), (1, 0), (1, 1))
 
@@ -762,7 +774,7 @@
     def spot(of):
         return lax.rem(of, plane) * depth + of // plane
 
-    down_swap = remote(s.wd.at[:, core], s.wd.at[:, core], s.swap_send.at[4], s.swap_recv.at[4], place.partner)
+    down_swap = remote(s.wd.at[:, :, core], s.wd.at[:, :, core], s.swap_send.at[4], s.swap_recv.at[4], place.partner)
     waiting[24] = down_swap.wait_recv
 
     def arrived(view, recv):
@@ -863,12 +875,14 @@
         if b == BATCHES - 1:
             for index, turn in enumerate(peers):
                 wide_copy(index, place.on(z, *turn)).start()
-            for target in others():
-                down_copy(target).start()
-            sends.append(departed(s.wd.at[others_ds, core], s.down_send.at[0]))
+            for step in range(1, depth):
+                zo = place.sweep(step)
+                remote(*down_line(zo), s.down_send.at[0], s.down_recv.at[0], place.device(place.on(zo))).start()
+            sends.append(departed(s.transit.at[pl.ds(0, depth - 1)], s.down_send.at[0]))
+            sends.append(departed(s.wd.at[:, pl.ds(0, 3), 0], s.down_send.at[1]))
             sends.append(departed(s.wo.at[pl.ds(0, 3), 0], s.wide_send.at[0]))
             sends.append(departed(s.wo.at[pl.ds(0, 3), 0], s.pass_send.at[0]))
-            fetch(11, wd_hbm.at[:, pl.ds(pl.multiple_of(chip * lanes, lanes), lanes)], s.wd.at[chip, core])
+            fetch(11, *down_line(z))
             need(4, 5)
             own_normed = norm_rows(tokens_ref[...].astype(f32), gain1_ref[...])
             newk_ref[...] = dot(own_normed, s.wk[...]).astype(bf16)
@@ -900,7 +914,8 @@
                 if index == 0:
                     need(1)
                 wide_pass(index)
-        yield begin + 5.5
+            down_across()
+        yield begin + (5.5 if b == 0 else 6.5)
         arrived(line_view, s.line_recv.at[b])
         need(21)
         if b == 0:
@@ -917,8 +932,8 @@
         sends.append(gather.finish)
         yield from gather.steps()
         if b == 0:
-            need(11)
-            arrived(s.wd.at[others_ds, core], s.down_recv.at[0])
+            need(12)
+            arrived(s.wd.at[:, pl.ds(0, 3), core], s.down_recv.at[1])
             down_swap.start()
             sends.append(down_swap.wait_send)
         both = s.rows.at[b]
@@ -945,14 +960,6 @@
 
         yield gather.due(0)
         need(8, 9, 10)
-
-        if b == 0:
-
-            @pl.when((group == b) & (core == 0))
-            def _():
-                serve(1, True)
-
-            clock.spend(0.6)
         gather.rest(0)
 
         block = rows // 2
@@ -1010,11 +1017,9 @@
         def _():
             serve(0, True)
 
-        if b > 0:
-
-            @pl.when((group == b) & (core == 0))
-            def _():
-                serve(1, True)
+        @pl.when((group == b) & (core == 0))
+        def _():
+            serve(1, True)
 
         clock.spend(0.6)
 
@@ -1060,7 +1065,7 @@
 
             for c in (2 * piece, 2 * piece + 1):
                 at = slice(c * chunk, (c + 1) * chunk)
-                down = s.wd[c * (chips // 4) : (c + 1) * (chips // 4)].reshape(chunk, lanes)
+                down = s.wd[c * depth // 4 : (c + 1) * depth // 4].reshape(chunk, lanes)
                 value = jax.nn.sigmoid(logit_ref[:, at]) * dot_t(dense, down)
                 value = value.reshape(chips, seq, chunk)
 
@@ -1083,7 +1088,7 @@
         begin = clock.now
 
         for step in range(depth - 1, -1, -1):
-            yield begin + 2.5 + 0.8 * (depth - 1 - step)
+            yield begin + 5.0 + 0.2 * (depth - 1 - step)
             for piece in range(2):
                 first, second = (place.turn(a) for a in ORDERS[piece])
                 zo = place.sweep(step)
@@ -1097,11 +1102,11 @@
             return value + summand(piece, depth + 2 * zo + 1)
 
         for step in range(depth - 1, 0, -1):
-            yield begin + 5.2 + 0.8 * (depth - 1 - step)
+            yield begin + 8.0 + 0.2 * (depth - 1 - step)
             for piece in range(2):
                 zo = place.sweep(step)
                 staged(piece, folded(piece, zo), 3 * depth + step - 1, 3 * depth + z, 2 * depth, place.on(zo))
-        yield begin + 8.0
+        yield begin + 9.0
         for piece in range(2):
             at = columns_of(piece)
             value = slots1[chip, :, lanes + piece * half : lanes + (piece + 1) * half].astype(f32)
@@ -1109,7 +1114,7 @@
                 [slots3[k * plane + spot_me, z] for k in range(piece * depth // 2, (piece + 1) * depth // 2)], axis=1
             ).astype(f32)
             acc[spot(chip), :, at] = value + folded(piece, z)
-        yield begin + 11.0
+        yield begin + 13.0
         for piece in range(2):
             summands(piece, 3 * depth, depth - 1, 2 * depth)
             value = acc[spot(chip), :, columns_of(piece)]
@@ -1150,7 +1155,8 @@
         eg=pltpu.VMEM((width, fe), bf16),
         eu=pltpu.VMEM((width, fe), bf16),
         ed=pltpu.VMEM((fe, width), bf16),
-        wd=pltpu.VMEM((chips, 2, LANES // 2, LANES), bf16),
+        wd=pltpu.VMEM((depth, chips // depth, 2, LANES // 2, LANES), bf16),
+        transit=pltpu.VMEM((depth, LANES // 2, chips // depth * LANES), bf16),
         after=pltpu.VMEM((2 * LANES, 2 * LANES), bf16),
         bias=pltpu.VMEM((HEADS, LANES), f32),
         tiles=pltpu.VMEM((n, chips, seq, LANES), bf16),
@@ -1166,7 +1172,7 @@
         acc=pltpu.VMEM((n, chips, seq, width), f32),
         stage=pltpu.VMEM((n, 2, 4 * depth, seq, half), bf16),
         sums=pltpu.VMEM((n, 2, 4 * depth, seq, half), bf16),
-        local_sem=DMA((12,)),
+        local_sem=DMA((13,)),
         swap_send=DMA((5,)),
         swap_recv=DMA((5,)),
         gather_send=DMA((n, 2, 2)),
@@ -1179,8 +1185,8 @@
         pass_recv=DMA((1,)),
         tile_send=DMA((n,)),
         tile_recv=DMA((n,)),
-        down_send=DMA((1,)),
-        down_recv=DMA((1,)),
+        down_send=DMA((2,)),
+        down_recv=DMA((2,)),
         square_send=DMA((n,)),
         square_recv=DMA((n,)),
         row_send=DMA((n,)),
@@ -1233,7 +1239,7 @@
 def one_kernel(mesh):
     chips = mesh.shape["ep"] // 2
     depth, height, width = torus_of(chips)
-    return (height, width) == (2, 2) and chips * LANES == HEADS * HEAD_DIM and 4 * chips <= LANES and depth % 2 == 0 and 2 * chips == BATCHES * PER_GROUP
+    return (height, width) == (2, 2) and chips * LANES == HEADS * HEAD_DIM and 4 * chips <= LANES and depth % 4 == 0 and 2 * chips == BATCHES * PER_GROUP
 
 
 def solution(mesh):

time: 79.7 us -> 78 us (0.979)
  Pallas kernels: 78.9 us -> 77.2 us
    pallas_call x1, Pallas kernels: 77.4 us -> 75.7 us  [fused_shards(): pl.pallas_call(functools.partial(layer_kernel, chips, tuple(scratch)), ou...]
where the time goes in v1:
time: 78 us; the launch traced here: 77.8 us
  Pallas kernels  77.2 us (99%)
    pallas_call x1, Pallas kernels, fused_shards(): pl.pallas_call(functools.partial(layer_kernel, chips, tuple(scratch)), ou...  75.7 us

profile of v1, /device:TPU:0, one launch (start us, length us, event | category | flops | bytes accessed | tf_op | source)
XLA Modules:
  0.0 77.8 jit_solution(11974796304002872923)
XLA Ops:
  0.6 75.7 %layer.1 = (bf16[16,2048]{1,0:T(8,128)(2,1)}, bf16[16,128]{1,0:T(8,128)(2,1)}, bf16[16,128]{1,0:T(8,128)(2,1)}) custom-call(s32[16]{0:T(128)} %lens_ref.1, s32[16]{0:T(128)} %ids_ref.1, f32[32]{0:T(128)} %bias_ref.1, bf16[16,2048]{1,0:T(8,128)(2,1)} %tokens_ref.1, f32[1,2048]{1,0:T(1,128)} %bitcast.18, f32[1,2048]{1,0:T(1,128)} %bitcast.19, ...), custom_call_target="tpu_custom_call" | custom-call | tf_op jit(solution)/shard_map/layer/pallas_call | solution.py:1218
  76.3 1.5 %results.1 = (bf16[16,2048]{1,0:T(8,128)(2,1)}, bf16[16,128]{1,0:T(8,128)(2,1)}, bf16[16,128]{1,0:T(8,128)(2,1)}) custom-call(bf16[16,2048]{1,0:T(8,128)(2,1)} %get-tuple-element.6.a_ref, bf16[16,128]{1,0:T(8,128)(2,1)} %get-tuple-element.7.b_ref, bf16[16,128]{1,0:T(8,128)(2,1)} %get-tuple-element.8.c_ref), custom_call_target="tpu_custom_call" | custom-call | tf_op jit(solution)/shard_map/results/pallas_call | solution.py:1234

commit v2 on v1

--- a/solution.py
+++ b/solution.py
@@ -1011,7 +1011,7 @@
                 serve(c, False)
 
         clock.spend(1.0)
-        yield sent_at + 5.5
+        yield sent_at + (1.5 if b == 0 else 5.5)
 
         @pl.when((group == b) & (core == 1))
         def _():
@@ -1030,6 +1030,7 @@
                 departed(s.gift, s.gift_send.at[0])()
 
         sends.append(end_served)
+        yield sent_at + 5.5
 
         arrived(squares.at[others_ds], s.square_recv.at[b])
         total = squares[0]
@@ -1042,6 +1043,8 @@
         need(24)
 
         stage = s.stage.at[b]
+        if b > 0:
+            yield sent_at + 7.5
 
         def staged(piece, value, slot, index, recv, target):
             stage[piece, slot] = value.astype(bf16)
@@ -1088,7 +1091,7 @@
         begin = clock.now
 
         for step in range(depth - 1, -1, -1):
-            yield begin + 5.0 + 0.2 * (depth - 1 - step)
+            yield begin + (4.3 if b == 0 else 5.0) + 0.02 * (depth - 1 - step)
             for piece in range(2):
                 first, second = (place.turn(a) for a in ORDERS[piece])
                 zo = place.sweep(step)
@@ -1106,7 +1109,7 @@
             for piece in range(2):
                 zo = place.sweep(step)
                 staged(piece, folded(piece, zo), 3 * depth + step - 1, 3 * depth + z, 2 * depth, place.on(zo))
-        yield begin + 9.0
+        yield begin + 15.0
         for piece in range(2):
             at = columns_of(piece)
             value = slots1[chip, :, lanes + piece * half : lanes + (piece + 1) * half].astype(f32)
@@ -1114,7 +1117,7 @@
                 [slots3[k * plane + spot_me, z] for k in range(piece * depth // 2, (piece + 1) * depth // 2)], axis=1
             ).astype(f32)
             acc[spot(chip), :, at] = value + folded(piece, z)
-        yield begin + 13.0
+        yield begin + 20.0
         for piece in range(2):
             summands(piece, 3 * depth, depth - 1, 2 * depth)
             value = acc[spot(chip), :, columns_of(piece)]

time: 78 us -> 75.7 us (0.971)
  Pallas kernels: 77.2 us -> 74.8 us
    pallas_call x1, Pallas kernels: 75.7 us -> 73.4 us  [fused_shards(): pl.pallas_call(functools.partial(layer_kernel, chips, tuple(scratch)), ou...]
where the time goes in v2:
time: 75.7 us; the launch traced here: 75.5 us
  Pallas kernels  74.8 us (99%)
    pallas_call x1, Pallas kernels, fused_shards(): pl.pallas_call(functools.partial(layer_kernel, chips, tuple(scratch)), ou...  73.4 us

profile of v2, /device:TPU:0, one launch (start us, length us, event | category | flops | bytes accessed | tf_op | source)
XLA Modules:
  0.0 75.5 jit_solution(11345056052640937344)
XLA Ops:
  0.6 73.4 %layer.1 = (bf16[16,2048]{1,0:T(8,128)(2,1)}, bf16[16,128]{1,0:T(8,128)(2,1)}, bf16[16,128]{1,0:T(8,128)(2,1)}) custom-call(s32[16]{0:T(128)} %lens_ref.1, s32[16]{0:T(128)} %ids_ref.1, f32[32]{0:T(128)} %bias_ref.1, bf16[16,2048]{1,0:T(8,128)(2,1)} %tokens_ref.1, f32[1,2048]{1,0:T(1,128)} %bitcast.18, f32[1,2048]{1,0:T(1,128)} %bitcast.19, ...), custom_call_target="tpu_custom_call" | custom-call | tf_op jit(solution)/shard_map/layer/pallas_call | solution.py:1221
  74.0 1.5 %results.1 = (bf16[16,2048]{1,0:T(8,128)(2,1)}, bf16[16,128]{1,0:T(8,128)(2,1)}, bf16[16,128]{1,0:T(8,128)(2,1)}) custom-call(bf16[16,2048]{1,0:T(8,128)(2,1)} %get-tuple-element.6.a_ref, bf16[16,128]{1,0:T(8,128)(2,1)} %get-tuple-element.7.b_ref, bf16[16,128]{1,0:T(8,128)(2,1)} %get-tuple-element.8.c_ref), custom_call_target="tpu_custom_call" | custom-call | tf_op jit(solution)/shard_map/results/pallas_call | solution.py:1237
